TPU v7x, 128 devices: a whole 4x4x4 slice. The times are simulated.
128 devices in a mesh: ep: 128 (over z, y, x, core).
Axes of the slice: x: 4, y: 4, z: 4, core: 2. Of those that a mesh axis runs over, the one named last changes fastest.
Arguments:
- tokens: bfloat16 [512, 2048], P('ep'), may hold values from -6 to 6
- lengths: int32 [512], P('ep'), may hold values from 1 to 1023
- cache_keys: bfloat16 [512, 1024, 2, 128], P('ep')
- cache_values: bfloat16 [512, 1024, 2, 128], P('ep'), may hold values from -6 to 6
- query_w: bfloat16 [2048, 1024], replicated, may hold values from -0.125 to 0.125
- key_w: bfloat16 [2048, 256], replicated, may hold values from -0.125 to 0.125
- value_w: bfloat16 [2048, 256], replicated, may hold values from -0.125 to 0.125
- out_w: bfloat16 [1024, 2048], replicated, may hold values from -0.1875 to 0.1875
- mix_lambda: float32 [8], replicated, may hold values from 0.3 to 0.8
- head_gain: float32 [128], replicated, may hold values from 0.1 to 1.9
- attn_gain: float32 [2048], replicated, may hold values from 0.1 to 1.9
- ffn_gain: float32 [2048], replicated, may hold values from 0.1 to 1.9
- routes: int32 [512, 2], P('ep'), may hold values from 0 to 7, all different within a row; in each aligned block of 4 rows (0 to 3, 4 to 7, ...) at most 2 rows name the same one
- route_weights: float32 [512, 2], P('ep'), may hold values from 0.2 to 1
- exp_gate: bfloat16 [2048, 49152], P(None, 'ep'), may hold values from -0.125 to 0.125
- exp_up: bfloat16 [2048, 49152], P(None, 'ep'), may hold values from -0.125 to 0.125
- exp_down: bfloat16 [49152, 2048], P('ep'), may hold values from -0.078125 to 0.078125
- dense_gate: bfloat16 [128, 256, 352], P('ep'), may hold values from -0.125 to 0.125
- dense_up: bfloat16 [128, 256, 352], P('ep'), may hold values from -0.125 to 0.125
- dense_down: bfloat16 [128, 352, 256], P('ep'), may hold values from -0.078125 to 0.078125
- branch_gate: bfloat16 [2048], replicated, may hold values from -0.125 to 0.125
Outputs:
- output: bfloat16 [512, 2048], P('ep')
- new_keys: bfloat16 [512, 256], P('ep')
- new_values: bfloat16 [512, 256], P('ep')
Inputs may be any that keep to these rules, and one draw needn't show every extreme that they name: `routes`: each row names 2 different experts; among the 4 rows of one device no expert is named by more than 2 rows, a bound that some block reaches.
All inputs are finite; a program needn't handle non-finite values.
Results may differ from a plain program's by a relative error of at most 0.015.
Values may be sent and summed in bfloat16 or wider, within the bound.
A program may use at most 128 MiB of HBM per device.

v0:
```python
import jax
import jax.numpy as jnp
from jax import lax
from jax.sharding import PartitionSpec as P

HEADS = 8
KV_HEADS = 2
HEAD_DIM = 128
SEQ_DEV = 4
TOP_K = 2
SPLIT = 16


def sent_together(arrays, axis, split_dim, concat_dim, along):
    widths = [a.shape[along] for a in arrays]
    both = jnp.concatenate(arrays, axis=along)
    filled = lax.all_to_all(both, axis, split_axis=split_dim, concat_axis=concat_dim, tiled=True)
    return tuple(jnp.split(filled, [sum(widths[:k]) for k in range(1, len(widths))], axis=along))


def split_up(x, dim, peers):
    before, after = (x.shape[:dim], x.shape[dim + 1 :])
    return jnp.moveaxis(x.reshape(*before, peers, -1, *after), dim, 0)


def cut_rows(length, count):
    unit = 8 if length >= 8 * count else 1
    return [length // unit * k // count * unit for k in range(1, count)]


def in_order(tiles, dim):
    lengths = list(tiles.shape[1:])
    lengths[dim] *= tiles.shape[0]
    return jnp.moveaxis(tiles, 0, dim).reshape(lengths)


def exchange_in_pieces(x, axis, pieces, split_dim, concat_dim):
    tiles = split_up(x, split_dim, lax.axis_size(axis))
    cut = max(range(1, max(2, tiles.ndim - 1)), key=lambda d: tiles.shape[d])
    outs = []
    for piece in jnp.split(tiles, cut_rows(tiles.shape[cut], pieces), axis=cut):
        if piece.size:
            outs.append(lax.all_to_all(piece, axis, split_axis=0, concat_axis=0, tiled=True))
    return in_order(jnp.concatenate(outs, axis=cut), concat_dim)


def rms_norm(values, gain, epsilon):
    scale = lax.rsqrt(jnp.mean(values * values, axis=-1, keepdims=True) + epsilon)
    return values * scale * gain


def softmax_pair(scores, own_score, valid):
    masked = jnp.where(valid, scores, -jnp.inf)
    largest = jnp.maximum(jnp.max(masked, axis=-1), own_score)
    raised = jnp.where(valid, jnp.exp(scores - largest[..., None]), 0.0)
    own_raised = jnp.exp(own_score - largest)
    total = jnp.sum(raised, axis=-1) + own_raised
    return (raised / total[..., None], own_raised / total)


def swiglu_rows(chosen, w_gate, w_up, w_down):
    gate_part = jnp.dot(chosen, w_gate, preferred_element_type=jnp.float32)
    up_part = jnp.dot(chosen, w_up, preferred_element_type=jnp.float32)
    act = (jax.nn.silu(gate_part) * up_part).astype(jnp.bfloat16)
    return jnp.dot(act, w_down, preferred_element_type=jnp.float32)


def per_device(
    tokens,
    lengths,
    cache_keys,
    cache_values,
    query_w,
    key_w,
    value_w,
    out_w,
    mix_lambda,
    head_gain,
    attn_gain,
    ffn_gain,
    routes,
    route_weights,
    exp_gate,
    exp_up,
    exp_down,
    dense_gate,
    dense_up,
    dense_down,
    branch_gate,
):
    rows = tokens.shape[0]
    groups = HEADS // KV_HEADS
    half = HEAD_DIM // 2
    scale = (HEAD_DIM // 2) ** (-0.5)
    cache_len = cache_keys.shape[1]
    xfull = tokens.astype(jnp.float32)
    normed = rms_norm(xfull, attn_gain, 1e-06).astype(jnp.bfloat16)
    query = jnp.dot(normed, query_w, preferred_element_type=jnp.float32).astype(jnp.bfloat16)
    key_new = jnp.dot(normed, key_w, preferred_element_type=jnp.float32).astype(jnp.bfloat16)
    value_new = jnp.dot(normed, value_w, preferred_element_type=jnp.float32).astype(jnp.bfloat16)
    qheads = query.reshape(rows, KV_HEADS, groups, HEAD_DIM)
    knew = key_new.reshape(rows, KV_HEADS, HEAD_DIM)
    vnew = value_new.reshape(rows, KV_HEADS, HEAD_DIM)
    valid = (jnp.arange(cache_len, dtype=jnp.int32)[None, :] < lengths[:, None])[:, None, None, :]
    first = (
        jnp.einsum(
            "sgqd,spgd->sgqp",
            qheads[..., :half],
            cache_keys[..., :half],
            preferred_element_type=jnp.float32,
        )
        * scale
    )
    first_own = (
        jnp.einsum(
            "sgqd,sgd->sgq",
            qheads[..., :half],
            knew[..., :half],
            preferred_element_type=jnp.float32,
        )
        * scale
    )
    second = (
        jnp.einsum(
            "sgqd,spgd->sgqp",
            qheads[..., half:],
            cache_keys[..., half:],
            preferred_element_type=jnp.float32,
        )
        * scale
    )
    second_own = (
        jnp.einsum(
            "sgqd,sgd->sgq",
            qheads[..., half:],
            knew[..., half:],
            preferred_element_type=jnp.float32,
        )
        * scale
    )
    prob_one, own_one = softmax_pair(first, first_own, valid)
    prob_two, own_two = softmax_pair(second, second_own, valid)
    lam = mix_lambda.reshape(KV_HEADS, groups)
    weights = (prob_one - lam[None, :, :, None] * prob_two).astype(jnp.bfloat16)
    own_weights = (own_one - lam[None] * own_two).astype(jnp.bfloat16)
    mixed = jnp.einsum("sgqp,spgd->sgqd", weights, cache_values, preferred_element_type=jnp.float32)
    mixed = (
        mixed + own_weights.astype(jnp.float32)[..., None] * vnew.astype(jnp.float32)[:, :, None, :]
    )
    heads = rms_norm(mixed, head_gain, 1e-05).astype(jnp.bfloat16).reshape(rows, HEADS * HEAD_DIM)
    hidden_state = xfull + jnp.dot(heads, out_w, preferred_element_type=jnp.float32)
    ffn_in = rms_norm(hidden_state, ffn_gain, 1e-06).astype(jnp.bfloat16)
    devices = lax.axis_size("ep")
    experts = devices // SPLIT
    row_blocks = devices // SPLIT
    capacity = min(SEQ_DEV, max(2, SEQ_DEV * TOP_K * 2 // experts))
    slots = jnp.arange(capacity, dtype=jnp.int32)
    all_rows = lax.all_gather(ffn_in, "ep", axis=0, tiled=True)
    gate = jax.nn.sigmoid(jnp.dot(ffn_in, branch_gate, preferred_element_type=jnp.float32))
    position = lax.axis_index("ep")
    row_span = dense_gate.shape[1]
    col_span = dense_gate.shape[2]
    row_block = position // SPLIT
    columns = lax.dynamic_slice_in_dim(all_rows, row_block * row_span, row_span, 1)
    gate_tile = jnp.dot(columns, dense_gate[0], preferred_element_type=jnp.float32).reshape(
        devices, rows, col_span
    )
    up_tile = jnp.dot(columns, dense_up[0], preferred_element_type=jnp.float32).reshape(
        devices, rows, col_span
    )
    gate_in, up_in = tuple(
        (
            part.astype(jnp.float32)
            for part in sent_together(
                (gate_tile.astype(jnp.bfloat16), up_tile.astype(jnp.bfloat16)), "ep", 0, 0, 1
            )
        )
    )
    gate_sum = jnp.sum(gate_in.reshape(row_blocks, SPLIT, rows, col_span), axis=0)
    up_sum = jnp.sum(up_in.reshape(row_blocks, SPLIT, rows, col_span), axis=0)
    own_act = (jax.nn.silu(gate_sum) * up_sum).astype(jnp.bfloat16)
    outgoing_act = jnp.tile(own_act, (row_blocks, 1, 1))
    act_in = lax.all_to_all(outgoing_act, "ep", split_axis=0, concat_axis=0, tiled=True)
    down_tile = jnp.dot(
        act_in.reshape(devices * rows, col_span), dense_down[0], preferred_element_type=jnp.float32
    )
    down_in = lax.all_to_all(
        down_tile.reshape(devices, rows, row_span).astype(jnp.bfloat16),
        "ep",
        split_axis=0,
        concat_axis=0,
        tiled=True,
    ).astype(jnp.float32)
    down_sum = jnp.sum(down_in.reshape(row_blocks, SPLIT, rows, row_span), axis=1)
    dense = jnp.transpose(down_sum, (1, 0, 2)).reshape(rows, row_blocks * row_span)
    expert_ids = jnp.arange(experts, dtype=jnp.int32)
    match = routes[None, :, :] == expert_ids[:, None, None]
    weight = jnp.sum(jnp.where(match, route_weights[None], 0.0), axis=-1)
    hit = jnp.any(match, axis=-1).astype(jnp.int32)
    rank = jnp.cumsum(hit, axis=1) - 1
    select = (hit[:, None, :] == 1) & (rank[:, None, :] == slots[None, :, None])
    chosen = jnp.einsum(
        "ecs,sd->ecd", select.astype(jnp.bfloat16), ffn_in, preferred_element_type=jnp.float32
    ).astype(jnp.bfloat16)
    outgoing = jnp.repeat(chosen, SPLIT, axis=0)
    incoming = lax.all_to_all(outgoing, "ep", split_axis=0, concat_axis=0, tiled=True)
    sources = incoming.shape[0]
    taken = incoming.shape[1]
    result = swiglu_rows(incoming.reshape(sources * taken, -1), exp_gate, exp_up, exp_down)
    returned = exchange_in_pieces(
        result.reshape(sources, taken, -1).astype(jnp.bfloat16), "ep", 2, 0, 0
    ).astype(jnp.float32)
    summed = jnp.sum(returned.reshape(experts, SPLIT, capacity, -1), axis=1)
    weighted = select.astype(jnp.float32) * weight[:, None, :]
    routed = jnp.einsum("ecs,ecd->sd", weighted, summed, precision=lax.Precision.HIGHEST)
    output = (hidden_state + routed + gate[:, None] * dense).astype(jnp.bfloat16)
    return (output, key_new, value_new)


def solution(mesh):
    placed = (
        P("ep", None),
        P("ep"),
        P("ep", None, None, None),
        P("ep", None, None, None),
        P(),
        P(),
        P(),
        P(),
        P(),
        P(),
        P(),
        P(),
        P("ep", None),
        P("ep", None),
        P(None, "ep"),
        P(None, "ep"),
        P("ep", None),
        P("ep", None, None),
        P("ep", None, None),
        P("ep", None, None),
        P(),
    )
    return jax.shard_map(
        per_device,
        mesh=mesh,
        in_specs=placed,
        out_specs=(P("ep", None), P("ep", None), P("ep", None)),
        check_vma=False,
    )
```

profile of v0, /device:TPU:0, one launch (start us, length us, event | category | flops | bytes accessed | tf_op | source)
XLA Modules:
  0.0 198.4 jit_solution(3395068889452520648)
XLA Ops:
  8.2 2.9 %convolution_convert_fusion.5 = bf16[4,1024]{1,0:T(4,128)(2,1)S(1)} fusion(bf16[2048,1024]{1,0:T(8,128)(2,1)} %param.25, bf16[4,2048]{1,0:T(4,128)(2,1)} %param.21, f32[2048]{0:T(1024)} %param.31, f32[4]{0:T(128)S(1)} %add_rsqrt_fusion.2), kind=kOutput, calls=%fused_computation.22 | convolution fusion | flops 16814080 | bytes 4227088 | tf_op jit(solution)/shard_map/dot_general | solution.py:98
  11.3 6.8 %fusion.79 = (bf16[4,1024,2,64]{3,2,1,0:T(2,128)(2,1)}, bf16[4,1024,2,64]{3,2,1,0:T(2,128)(2,1)}) fusion(bf16[4,1024,2,128]{3,2,1,0:T(2,128)(2,1)} %param.23), kind=kLoop, calls=%fused_computation.114 | loop fusion | bytes 4194304 | tf_op jit(solution)/shard_map/slice | solution.py:127
  23.5 3.0 %multiply_reduce_fusion = (f32[4]{0:T(128)S(1)}, f32[4,2048]{1,0:T(4,128)S(1)}) fusion(bf16[4,1024]{1,0:T(4,128)(2,1)S(1)} %reshape.161, bf16[1024,2048]{1,0:T(8,128)(2,1)} %param.28, bf16[4,2048]{1,0:T(4,128)(2,1)S(1)} %copy-done.6), kind=kOutput, calls=%fused_computation.70 | convolution fusion | flops 16809980 | bytes 4251664 | tf_op jit(solution)/shard_map/dot_general | solution.py:151
  29.3 11.9 %all-to-all-start = ((bf16[128,2,2048]{2,1,0:T(2,128)(2,1)}), bf16[128,2,2048]{2,1,0:T(2,128)(2,1)}, u32[]{:S(2)}, u32[]{:S(2)}) async-start(bf16[128,2,2048]{2,1,0:T(2,128)(2,1)} %bitcast.7), calls=%async_computation | async-start | bytes 2097152 | tf_op jit(solution)/shard_map/all_to_all | solution.py:206
  41.3 18.7 %all-to-all-done = bf16[128,2,2048]{2,1,0:T(2,128)(2,1)} async-done(((bf16[128,2,2048]{2,1,0:T(2,128)(2,1)}), bf16[128,2,2048]{2,1,0:T(2,128)(2,1)}, u32[]{:S(2)}, u32[]{:S(2)}) %all-to-all-start) | async-done | bytes 1048608 | tf_op jit(solution)/shard_map/all_to_all | solution.py:206
  61.4 2.9 %fusion.82 = f32[256,384]{1,0:T(8,128)} fusion(bf16[256,2048]{1,0:T(8,128)(2,1)S(1)} %reshape.163, bf16[2048,384]{1,0:T(8,128)(2,1)} %param.35), kind=kOutput, calls=%fused_computation.117 | convolution fusion | flops 402653184 | bytes 3014656 | tf_op jit(solution)/shard_map/dot_general | solution.py:62
  64.3 4.4 %convolution_convert_fusion = bf16[256,2048]{1,0:T(8,128)(2,1)} fusion(bf16[384,2048]{1,0:T(8,128)(2,1)} %param.37, bf16[256,2048]{1,0:T(8,128)(2,1)S(1)} %reshape.163, bf16[2048,384]{1,0:T(8,128)(2,1)} %param.36, f32[256,384]{1,0:T(8,128)} %fusion.82), kind=kOutput, calls=%fused_computation | convolution fusion | flops 806420480 | bytes 5636096 | tf_op jit(solution)/shard_map/dot_general | solution.py:65
  70.4 2.5 %fusion.80 = (bf16[128,1,1,2048]{3,2,1,0:T(2,128)(2,1)}, bf16[128,1,1,2048]{3,2,1,0:T(2,128)(2,1)}) fusion(bf16[128,1,2,2048]{3,2,1,0:T(2,128)(2,1)S(1)} %bitcast.73), kind=kLoop, calls=%fused_computation.115 | loop fusion | bytes 2097152 | tf_op jit(solution)/shard_map/split | solution.py:41
  73.4 4.7 %reduce = bf16[128,2048]{1,0:T(8,128)(2,1)S(1)} reduce(bf16[128,1,1,2048]{3,2,1,0:T(2,128)(2,1)} %get-tuple-element.8, bf16[]{:T(256)} %broadcast.142), dimensions={1,2}, to_apply=%get-tuple-element.8.reduce_sub_computation | reduce | bytes 1048578 | tf_op jit(solution)/shard_map/split | solution.py:41
  79.3 5.7 %all-to-all-start.2 = ((bf16[128,2,1024]{2,1,0:T(2,128)(2,1)}), bf16[128,2,1024]{2,1,0:T(2,128)(2,1)}, u32[]{:S(2)}, u32[]{:S(2)}) async-start(bf16[128,2,1024]{2,1,0:T(2,128)(2,1)} %reshape.192), calls=%async_computation.2 | async-start | bytes 1048576 | tf_op jit(solution)/shard_map/all_to_all | solution.py:43
  85.1 18.9 %all-gather.3.cloned.1.call-done = bf16[128,4,2048]{2,1,0:T(4,128)(2,1)} async-done(((bf16[1,4,2048]{2,1,0:T(4,128)(2,1)}), bf16[128,4,2048]{2,1,0:T(4,128)(2,1)}) %all-gather.3.cloned.1.call-update) | async-done | bytes 2097168 | tf_op jit(solution)/shard_map/all_gather | solution.py:158
  104.0 4.0 %reshape.180 = bf16[512,2048]{1,0:T(8,128)(2,1)} reshape(bf16[128,4,2048]{2,1,0:T(4,128)(2,1)} %all-gather.3.cloned.1.call-done) | data formatting | bytes 4194304
  113.0 7.1 %all-to-all-start.3 = ((bf16[128,8,352]{2,1,0:T(8,128)(2,1)}), bf16[128,8,352]{2,1,0:T(8,128)(2,1)}, u32[]{:S(2)}, u32[]{:S(2)}) async-start(bf16[128,8,352]{2,1,0:T(8,128)(2,1)} %copy.84), calls=%async_computation.3 | async-start | bytes 1572864 | tf_op jit(solution)/shard_map/all_to_all | solution.py:17
  120.1 4.4 %reduce.1 = bf16[128,2048]{1,0:T(8,128)(2,1)} reduce(bf16[128,1,1,2048]{3,2,1,0:T(2,128)(2,1)S(1)} %copy-done.1, bf16[]{:T(256)} %broadcast.142), dimensions={1,2}, to_apply=%get-tuple-element.7.reduce_sub_computation | reduce | bytes 1048578 | tf_op jit(solution)/shard_map/split | solution.py:41
  126.8 9.1 %all-to-all-done.3 = bf16[128,8,352]{2,1,0:T(8,128)(2,1)} async-done(((bf16[128,8,352]{2,1,0:T(8,128)(2,1)}), bf16[128,8,352]{2,1,0:T(8,128)(2,1)}, u32[]{:S(2)}, u32[]{:S(2)}) %all-to-all-start.3) | async-done | bytes 720928 | tf_op jit(solution)/shard_map/all_to_all | solution.py:17
  135.9 4.6 %all-to-all-start.1 = ((bf16[128,2,1024]{2,1,0:T(2,128)(2,1)}), bf16[128,2,1024]{2,1,0:T(2,128)(2,1)S(1)}, u32[]{:S(2)}, u32[]{:S(2)}) async-start(bf16[128,2,1024]{2,1,0:T(2,128)(2,1)} %reshape.194), calls=%async_computation.1 | async-start | bytes 1048576 | tf_op jit(solution)/shard_map/all_to_all | solution.py:43
  143.6 10.4 %all-to-all-done.1 = bf16[128,2,1024]{2,1,0:T(2,128)(2,1)S(1)} async-done(((bf16[128,2,1024]{2,1,0:T(2,128)(2,1)}), bf16[128,2,1024]{2,1,0:T(2,128)(2,1)S(1)}, u32[]{:S(2)}, u32[]{:S(2)}) %all-to-all-start.1) | async-done | bytes 524320 | tf_op jit(solution)/shard_map/all_to_all | solution.py:43
  154.0 5.7 %all-to-all-start.4 = ((bf16[128,4,352]{2,1,0:T(4,128)(2,1)}), bf16[128,4,352]{2,1,0:T(4,128)(2,1)}, u32[]{:S(2)}, u32[]{:S(2)}) async-start(bf16[128,4,352]{2,1,0:T(4,128)(2,1)} %copy.87), calls=%async_computation.4 | async-start | bytes 786432 | tf_op jit(solution)/shard_map/all_to_all | solution.py:183
  159.9 3.6 %reshape.193 = bf16[128,1,1,2048]{3,2,1,0:T(2,128)(2,1)S(1)} reshape(bf16[128,2,1024]{2,1,0:T(2,128)(2,1)} %all-to-all-done.2) | data formatting | bytes 1048576
  163.5 4.4 %reshape.195 = bf16[128,1,1,2048]{3,2,1,0:T(2,128)(2,1)} reshape(bf16[128,2,1024]{2,1,0:T(2,128)(2,1)} %copy-done.2) | data formatting | bytes 1048576
  167.9 3.5 %all-to-all-done.4 = bf16[128,4,352]{2,1,0:T(4,128)(2,1)} async-done(((bf16[128,4,352]{2,1,0:T(4,128)(2,1)}), bf16[128,4,352]{2,1,0:T(4,128)(2,1)}, u32[]{:S(2)}, u32[]{:S(2)}) %all-to-all-start.4) | async-done | bytes 360480 | tf_op jit(solution)/shard_map/all_to_all | solution.py:183
  173.7 6.2 %all-to-all-start.5 = ((bf16[128,4,256]{2,1,0:T(4,128)(2,1)}), bf16[128,4,256]{2,1,0:T(4,128)(2,1)S(1)}, u32[]{:S(2)}, u32[]{:S(2)}) async-start(bf16[128,4,256]{2,1,0:T(4,128)(2,1)} %copy.89), calls=%async_computation.5 | async-start | bytes 524288 | tf_op jit(solution)/shard_map/all_to_all | solution.py:187
  179.8 3.5 %pad_maximum_fusion = bf16[128,1,2,2048]{3,2,1,0:T(2,128)(2,1)S(1)} fusion(bf16[128,1,1,2048]{3,2,1,0:T(2,128)(2,1)S(1)} %reshape.193, bf16[128,1,1,2048]{3,2,1,0:T(2,128)(2,1)} %reshape.195), kind=kLoop, calls=%fused_computation.30 | loop fusion | flops 2097152 | bytes 2097152 | tf_op jit(solution)/shard_map/concatenate | solution.py:44
  184.2 6.4 %all-to-all-done.5 = bf16[128,4,256]{2,1,0:T(4,128)(2,1)S(1)} async-done(((bf16[128,4,256]{2,1,0:T(4,128)(2,1)}), bf16[128,4,256]{2,1,0:T(4,128)(2,1)S(1)}, u32[]{:S(2)}, u32[]{:S(2)}) %all-to-all-start.5) | async-done | bytes 262176 | tf_op jit(solution)/shard_map/all_to_all | solution.py:187
  (99 shorter events, 28.9 us)
Async XLA Ops:
  7.2 15.6 %copy-start = (bf16[4,1024,2,128]{3,2,1,0:T(2,128)(2,1)S(1)}, bf16[4,1024,2,128]{3,2,1,0:T(2,128)(2,1)}, u32[]{:S(2)}) copy-start(bf16[4,1024,2,128]{3,2,1,0:T(2,128)(2,1)} %param.24) | copy-start | bytes 6291460
  7.2 96.8 %all-gather.3.cloned.1.call-start = ((), (), s32[]{:S(2)}) async-start(), calls=%async_computation.6 | async-start | bytes 2113536 | tf_op jit(solution)/shard_map/all_gather | solution.py:158
  8.2 2.9 %copy-start.17 = (s32[4]{0:T(128)S(1)}, s32[4]{0:T(128)}, u32[]{:S(2)}) copy-start(s32[4]{0:T(128)} %param.22) | copy-start | bytes 52
  11.3 6.8 %copy-start.4 = (bf16[2048,256]{1,0:T(8,128)(2,1)S(1)}, bf16[2048,256]{1,0:T(8,128)(2,1)}, u32[]{:S(2)}) copy-start(bf16[2048,256]{1,0:T(8,128)(2,1)} %param.26) | copy-start | bytes 3145732
  11.3 6.8 %copy-start.6 = (bf16[4,2048]{1,0:T(4,128)(2,1)S(1)}, bf16[4,2048]{1,0:T(4,128)(2,1)}, u32[]{:S(2)}) copy-start(bf16[4,2048]{1,0:T(4,128)(2,1)} %param.21) | copy-start | bytes 49156
  11.3 6.8 %copy-start.9 = (f32[2048]{0:T(1024)S(1)}, f32[2048]{0:T(1024)}, u32[]{:S(2)}) copy-start(f32[2048]{0:T(1024)} %param.31) | copy-start | bytes 24580
  11.3 7.5 %copy-start.18 = (f32[8]{0:T(128)S(1)}, f32[8]{0:T(128)}, u32[]{:S(2)}) copy-start(f32[8]{0:T(128)} %param.29) | copy-start | bytes 100
  11.3 7.6 %copy-start.5 = (bf16[2048,256]{1,0:T(8,128)(2,1)S(1)}, bf16[2048,256]{1,0:T(8,128)(2,1)}, u32[]{:S(2)}) copy-start(bf16[2048,256]{1,0:T(8,128)(2,1)} %param.27) | copy-start | bytes 3145732
  18.4 4.1 %copy-start.12 = (bf16[4,256]{1,0:T(4,128)(2,1)}, bf16[4,256]{1,0:T(4,128)(2,1)S(1)}, u32[]{:S(2)}) copy-start(bf16[4,256]{1,0:T(4,128)(2,1)S(1)} %convolution_convert_fusion.7) | copy-start | bytes 6148
  19.1 3.3 %copy-start.11 = (bf16[4,256]{1,0:T(4,128)(2,1)}, bf16[4,256]{1,0:T(4,128)(2,1)S(1)}, u32[]{:S(2)}) copy-start(bf16[4,256]{1,0:T(4,128)(2,1)S(1)} %convolution_convert_fusion.6) | copy-start | bytes 6148
  23.5 3.0 %copy-start.10 = (f32[2048]{0:T(1024)S(1)}, f32[2048]{0:T(1024)}, u32[]{:S(2)}) copy-start(f32[2048]{0:T(1024)} %param.32) | copy-start | bytes 24580
  23.5 3.7 %copy-start.14 = (s32[4,2]{0,1:T(2,128)S(1)}, s32[4,2]{0,1:T(2,128)}, u32[]{:S(2)}) copy-start(s32[4,2]{0,1:T(2,128)} %param.33) | copy-start | bytes 100
  29.3 30.6 %all-to-all-start = ((bf16[128,2,2048]{2,1,0:T(2,128)(2,1)}), bf16[128,2,2048]{2,1,0:T(2,128)(2,1)}, u32[]{:S(2)}, u32[]{:S(2)}) async-start(bf16[128,2,2048]{2,1,0:T(2,128)(2,1)} %bitcast.7), calls=%async_computation | async-start | bytes 2097152 | tf_op jit(solution)/shard_map/all_to_all | solution.py:206
  79.3 33.6 %all-to-all-start.2 = ((bf16[128,2,1024]{2,1,0:T(2,128)(2,1)}), bf16[128,2,1024]{2,1,0:T(2,128)(2,1)}, u32[]{:S(2)}, u32[]{:S(2)}) async-start(bf16[128,2,1024]{2,1,0:T(2,128)(2,1)} %reshape.192), calls=%async_computation.2 | async-start | bytes 1048576 | tf_op jit(solution)/shard_map/all_to_all | solution.py:43
  85.1 23.9 %copy-start.7 = (bf16[1,256,352]{1,2,0:T(8,128)(2,1)S(1)}, bf16[1,256,352]{1,2,0:T(8,128)(2,1)}, u32[]{:S(2)}) copy-start(bf16[1,256,352]{1,2,0:T(8,128)(2,1)} %param.39) | copy-start | bytes 540676
  85.1 24.2 %copy-start.8 = (bf16[1,256,352]{1,2,0:T(8,128)(2,1)S(1)}, bf16[1,256,352]{1,2,0:T(8,128)(2,1)}, u32[]{:S(2)}) copy-start(bf16[1,256,352]{1,2,0:T(8,128)(2,1)} %param.38) | copy-start | bytes 540676
  109.6 10.5 %copy-start.1 = (bf16[128,1,1,2048]{3,2,1,0:T(2,128)(2,1)S(1)}, bf16[128,1,1,2048]{3,2,1,0:T(2,128)(2,1)}, u32[]{:S(2)}) copy-start(bf16[128,1,1,2048]{3,2,1,0:T(2,128)(2,1)} %get-tuple-element.7) | copy-start | bytes 1572868
  113.0 22.9 %all-to-all-start.3 = ((bf16[128,8,352]{2,1,0:T(8,128)(2,1)}), bf16[128,8,352]{2,1,0:T(8,128)(2,1)}, u32[]{:S(2)}, u32[]{:S(2)}) async-start(bf16[128,8,352]{2,1,0:T(8,128)(2,1)} %copy.84), calls=%async_computation.3 | async-start | bytes 1572864 | tf_op jit(solution)/shard_map/all_to_all | solution.py:17
  135.9 18.1 %all-to-all-start.1 = ((bf16[128,2,1024]{2,1,0:T(2,128)(2,1)}), bf16[128,2,1024]{2,1,0:T(2,128)(2,1)S(1)}, u32[]{:S(2)}, u32[]{:S(2)}) async-start(bf16[128,2,1024]{2,1,0:T(2,128)(2,1)} %reshape.194), calls=%async_computation.1 | async-start | bytes 1048576 | tf_op jit(solution)/shard_map/all_to_all | solution.py:43
  142.2 17.4 %copy-start.13 = (bf16[2048]{0:T(1024)(128)(2,1)S(1)}, bf16[2048]{0:T(1024)(128)(2,1)}, u32[]{:S(2)}) copy-start(bf16[2048]{0:T(1024)(128)(2,1)} %param.41) | copy-start | bytes 12292
  142.3 17.4 %copy-start.15 = (f32[4,2]{0,1:T(2,128)S(1)}, f32[4,2]{0,1:T(2,128)}, u32[]{:S(2)}) copy-start(f32[4,2]{0,1:T(2,128)} %param.34) | copy-start | bytes 100
  154.0 5.8 %copy-start.2 = (bf16[128,2,1024]{2,1,0:T(2,128)(2,1)}, bf16[128,2,1024]{2,1,0:T(2,128)(2,1)S(1)}, u32[]{:S(2)}) copy-start(bf16[128,2,1024]{2,1,0:T(2,128)(2,1)S(1)} %all-to-all-done.1) | copy-start | bytes 1572868
  154.0 17.4 %all-to-all-start.4 = ((bf16[128,4,352]{2,1,0:T(4,128)(2,1)}), bf16[128,4,352]{2,1,0:T(4,128)(2,1)}, u32[]{:S(2)}, u32[]{:S(2)}) async-start(bf16[128,4,352]{2,1,0:T(4,128)(2,1)} %copy.87), calls=%async_computation.4 | async-start | bytes 786432 | tf_op jit(solution)/shard_map/all_to_all | solution.py:183
  173.7 16.9 %all-to-all-start.5 = ((bf16[128,4,256]{2,1,0:T(4,128)(2,1)}), bf16[128,4,256]{2,1,0:T(4,128)(2,1)S(1)}, u32[]{:S(2)}, u32[]{:S(2)}) async-start(bf16[128,4,256]{2,1,0:T(4,128)(2,1)} %copy.89), calls=%async_computation.5 | async-start | bytes 524288 | tf_op jit(solution)/shard_map/all_to_all | solution.py:187
  (2 other events, 3.2 us)
Sparse Core Ops, SparseCore 0:
  27.3 76.5 all-gather.2
where the time goes:
time: 200 us; the launch traced here: 198 us
  waiting for transfers between devices  66.9 us (33%)
  starting transfers between devices  41.2 us (21%)
  local copies, waits for them, and re-layouts  37.7 us (19%)
  matrix products  21 us (10%)
  other arithmetic  17.1 us (9%)
  between operations  14.5 us (7%)
    all_gather x1, waiting for transfers between devices, per_device(): all_rows = lax.all_gather(ffn_in, 'ep', axis=0, tiled=True)  18.9 us
    all_to_all x1, waiting for transfers between devices, per_device(): lax.all_to_all(outgoing, 'ep', split_axis=0, concat_axis=0, tiled=True)  18.7 us
    unnamed x46, local copies, waits for them, and re-layouts  15.6 us
    all_to_all x1, starting transfers between devices, per_device(): lax.all_to_all(outgoing, 'ep', split_axis=0, concat_axis=0, tiled=True)  11.9 us
    all_to_all x2, waiting for transfers between devices, exchange_in_pieces(): lax.all_to_all(piece, axis, split_axis=0, concat_axis=0, tiled=True)  10.4 us
    all_to_all x2, starting transfers between devices, exchange_in_pieces(): lax.all_to_all(piece, axis, split_axis=0, concat_axis=0, tiled=True)  10.3 us
    split x2, other arithmetic, exchange_in_pieces(): jnp.split(tiles, cut_rows(tiles.shape[cut], pieces), axis=cut)  9.14 us
    all_to_all x1, waiting for transfers between devices, sent_together(): lax.all_to_all(both, axis, split_axis=split_dim, concat_axis=concat_dim,...  9.06 us
  transfers between devices with their start and end apart: 7, of which 6 were waited for; matrix products, arithmetic and copies ran while one was open for 27% of the time, Pallas kernels for 0%

commit v1 on v0

v1 whole, which is shorter than its diff:
```python
import jax
import jax.numpy as jnp
from jax import lax
from jax.experimental import pallas as pl
from jax.experimental.pallas import tpu as pltpu
from jax.sharding import PartitionSpec as P

BF = jnp.bfloat16
F32 = jnp.float32
MESH = pl.DeviceIdType.MESH
ALL = slice(None)
D = 2048
META = 128
HID = 384
UNITS = 44
PAD = 48
PARTS = ((0, 768, "xyz"), (768, 640, "yzx"), (1408, 640, "zxy"))
STRIDE = {"x": 2, "y": 8, "z": 32}
NT = (((1,), (1,)), ((), ()))


def pick(**at):
    return tuple(at.get(axis, ALL) for axis in "zyx")


def to_col(row):
    n = row.shape[1]
    same = lax.broadcasted_iota(jnp.int32, (n, n), 0) == lax.broadcasted_iota(jnp.int32, (n, n), 1)
    return jnp.sum(jnp.where(same, jnp.broadcast_to(row, (n, n)), 0.0), axis=1, keepdims=True)


def kernel(
    tokens, lengths, keys, values, query_w, key_w, value_w, out_w, mix_lambda, head_gain,
    attn_gain, ffn_gain, routes, route_weights, exp_gate, exp_up, exp_down,
    dense_gate, dense_up, dense_down, branch_gate,
    out, new_keys, new_values,
    tok_v, len_v, k_v, v_v, wq_v, wk_v, wv_v, wo_v, lam_v, hg_v, ag_v, fg_v, rt_v, rw_v, bg_v,
    w1, w2, dgu, dg_v, du_v, dd_v, ds, qs, hs, xa, xf, act, pd, rs0, pf, sb1, rb1, sb2, rb2, sb3, rb3,
    load_sem, small_sem, w_sem, own_sem,
    ds_send, ds_recv, ag_send, ag_recv, dx_send, dx_recv, rd_send, rd_recv, rs_send, rs_recv,
):
    me = lax.axis_index("ep")
    core = lax.rem(me, 2)
    coord = {
        "x": lax.rem(lax.div(me, 2), 4),
        "y": lax.rem(lax.div(me, 8), 4),
        "z": lax.div(me, 32),
    }
    block = lax.div(me, 16)
    column = lax.rem(me, 16)
    partner = me + 1 - 2 * core

    def along(axis, k):
        there = lax.rem(coord[axis] + k, 4)
        return me + (there - coord[axis]) * STRIDE[axis], there

    barrier = pltpu.get_barrier_semaphore()
    friends = [partner]
    for axis in "xyz":
        for k in (1, 2, 3):
            friends.append(along(axis, k)[0])
    y_there = lax.rem(coord["y"] + 2, 4)
    for k in (1, 2, 3):
        z_there = lax.rem(coord["z"] + k, 4)
        friends.append(me + (z_there - coord["z"]) * 32 + (y_there - coord["y"]) * 8)
    for friend in friends:
        pl.semaphore_signal(barrier, inc=1, device_id=(friend,), device_id_type=MESH)

    def load(src, dst, sem):
        copy = pltpu.make_async_copy(src, dst, sem)
        copy.start()
        return copy

    small = [
        load(src, dst, small_sem.at[i])
        for i, (src, dst) in enumerate(
            (
                (tokens, tok_v), (attn_gain, ag_v), (dense_gate.at[0], dg_v), (dense_up.at[0], du_v),
                (dense_down.at[0], dd_v), (lengths, len_v), (mix_lambda, lam_v), (head_gain, hg_v),
                (ffn_gain, fg_v), (routes, rt_v), (route_weights, rw_v), (branch_gate, bg_v),
            )
        )
    ]
    step = D // 4
    qkv_loads = []
    for i in range(4):
        rows = pl.ds(i * step, step)
        qkv_loads.append(
            [
                load(query_w.at[rows], wq_v.at[rows], load_sem.at[3 * i]),
                load(key_w.at[rows], wk_v.at[rows], load_sem.at[3 * i + 1]),
                load(value_w.at[rows], wv_v.at[rows], load_sem.at[3 * i + 2]),
            ]
        )
    k_loads = [load(keys.at[s], k_v.at[s], load_sem.at[12 + s]) for s in range(4)]
    v_loads = [load(values.at[s], v_v.at[s], load_sem.at[16 + s]) for s in range(4)]
    o_load = load(out_w, wo_v, load_sem.at[20])
    w_loads = []
    for n in range(3):
        cols = pl.ds(n * 128, 128)
        w_loads.append(load(exp_gate.at[:, cols], w1.at[n, :, pl.ds(0, 128)], w_sem.at[2 * n]))
        w_loads.append(load(exp_up.at[:, cols], w1.at[n, :, pl.ds(128, 128)], w_sem.at[2 * n + 1]))
    w_loads.append(load(exp_down, w2.at[pl.ds(0, HID)], w_sem.at[6]))

    dgu[:, PAD:, :] = jnp.zeros((2, 128 - PAD, D), BF)
    w2[HID + PAD :, :] = jnp.zeros((128 - PAD, D), BF)
    row_i = lax.broadcasted_iota(jnp.int32, (PAD, 352), 0)
    col_i = lax.broadcasted_iota(jnp.int32, (PAD, 352), 1)
    for i in (2, 3, 4):
        small[i].wait()
    choose = jnp.concatenate(
        [
            jnp.where((col_i == row_i + UNITS * j) & (row_i < UNITS), 1.0, 0.0)
            for j in range(8)
        ],
        axis=0,
    ).astype(BF)
    ds[:, 0] = lax.dot_general(choose, dg_v[...], NT, preferred_element_type=F32).astype(BF).reshape(8, PAD, 256)
    ds[:, 1] = lax.dot_general(choose, du_v[...], NT, preferred_element_type=F32).astype(BF).reshape(8, PAD, 256)
    ds[:, 2] = jnp.dot(choose, dd_v[...], preferred_element_type=F32).astype(BF).reshape(8, PAD, 256)

    small[0].wait()
    small[1].wait()
    x = tok_v[...].astype(F32)
    normed = (x * lax.rsqrt(jnp.mean(x * x, axis=1, keepdims=True) + 1e-6) * ag_v[...]).astype(BF)

    pl.semaphore_wait(barrier, len(friends))
    own_cols = pl.ds(pl.multiple_of(block * 256, 256), 256)
    sent = []
    for k in range(1, 8):
        there = lax.rem(block + k, 8)
        for j, (src, dst) in enumerate(
            (
                (ds.at[there, pl.ds(0, 2)], dgu.at[:, pl.ds(0, PAD), own_cols]),
                (ds.at[there, 2], w2.at[pl.ds(HID, PAD), own_cols]),
            )
        ):
            copy = pltpu.make_async_remote_copy(
                src_ref=src, dst_ref=dst, send_sem=ds_send.at[j, k - 1], recv_sem=ds_recv.at[j, k - 1],
                device_id=(there * 16 + column,), device_id_type=MESH,
            )
            copy.start()
            sent.append(copy)
    own_loads = [
        load(ds.at[block, pl.ds(0, 2)], dgu.at[:, pl.ds(0, PAD), own_cols], own_sem.at[0]),
        load(ds.at[block, 2], w2.at[pl.ds(HID, PAD), own_cols], own_sem.at[1]),
    ]

    query = jnp.zeros((4, 1024), F32)
    key = jnp.zeros((4, 256), F32)
    value = jnp.zeros((4, 256), F32)
    for i in range(4):
        for copy in qkv_loads[i]:
            copy.wait()
        part = normed[:, i * step : (i + 1) * step]
        rows = pl.ds(i * step, step)
        query += jnp.dot(part, wq_v[rows, :], preferred_element_type=F32)
        key += jnp.dot(part, wk_v[rows, :], preferred_element_type=F32)
        value += jnp.dot(part, wv_v[rows, :], preferred_element_type=F32)
    key = key.astype(BF)
    value = value.astype(BF)
    new_keys[...] = key
    new_values[...] = value
    key = key.astype(F32)
    value = value.astype(F32)
    query = query.astype(BF).astype(F32)
    for h in range(8):
        qs[h] = query[:, h * 128 : (h + 1) * 128]

    for i in range(5, 12):
        small[i].wait()
    lam = to_col(lam_v[...])
    row8 = lax.broadcasted_iota(jnp.int32, (8, 128), 0)
    lane8 = lax.broadcasted_iota(jnp.int32, (8, 128), 1)
    row16 = lax.rem(lax.broadcasted_iota(jnp.int32, (16, 2048), 0), 8)
    spot = lax.broadcasted_iota(jnp.int32, (16, 2048), 1)
    matching = lax.rem(spot, 2) == lax.div(row16, 4)
    for s in range(4):
        heads_q = qs[:, s, :]
        q16 = jnp.concatenate(
            [jnp.where(lane8 < 64, heads_q, 0.0), jnp.where(lane8 >= 64, heads_q, 0.0)], axis=0
        )
        own_key = jnp.where(row8 < 4, key[s : s + 1, :128], key[s : s + 1, 128:])
        own_value = jnp.where(row8 < 4, value[s : s + 1, :128], value[s : s + 1, 128:])
        k_loads[s].wait()
        scores = lax.dot_general(q16.astype(BF), k_v[s], NT, preferred_element_type=F32) * 0.125
        own = jnp.sum(q16 * jnp.concatenate([own_key, own_key], axis=0), axis=1, keepdims=True) * 0.125
        valid = matching & (spot < 2 * len_v[0:1, s : s + 1])
        largest = jnp.maximum(jnp.max(jnp.where(valid, scores, -jnp.inf), axis=1, keepdims=True), own)
        raised = jnp.where(valid, jnp.exp(scores - largest), 0.0)
        own_raised = jnp.exp(own - largest)
        total = jnp.sum(raised, axis=1, keepdims=True) + own_raised
        prob = raised / total
        own_prob = own_raised / total
        weights = (prob[:8] - lam * prob[8:]).astype(BF)
        own_weight = (own_prob[:8] - lam * own_prob[8:]).astype(BF).astype(F32)
        v_loads[s].wait()
        mixed = jnp.dot(weights, v_v[s], preferred_element_type=F32) + own_weight * own_value
        mixed = mixed * lax.rsqrt(jnp.mean(mixed * mixed, axis=1, keepdims=True) + 1e-5) * hg_v[...]
        hs[s] = mixed
    heads = jnp.concatenate([hs[:, h, :] for h in range(8)], axis=1).astype(BF)
    o_load.wait()
    hidden = x + jnp.dot(heads, wo_v[...], preferred_element_type=F32)
    ffn_in = (
        hidden * lax.rsqrt(jnp.mean(hidden * hidden, axis=1, keepdims=True) + 1e-6) * fg_v[...]
    ).astype(BF)
    gate = jax.nn.sigmoid(
        jnp.sum(ffn_in.astype(F32) * bg_v[...].astype(F32), axis=1, keepdims=True)
    )
    lane4 = lax.broadcasted_iota(jnp.int32, (4, META), 1)
    expert4 = lax.rem(lane4, 8)
    scale = jnp.where(lane4 < 16, 0.0, gate)
    for j in range(2):
        named = to_col(rt_v[j : j + 1, :].astype(F32)).astype(jnp.int32)
        scale += jnp.where((expert4 == named) & (lane4 < 16), to_col(rw_v[j : j + 1, :]), 0.0)
    upper = scale.astype(BF).astype(F32)
    meta = jnp.where(
        (lane4 < 8) | (lane4 == 16), upper, jnp.where((lane4 < 16) | (lane4 == 17), scale - upper, 0.0)
    ).astype(BF)
    mine = (coord["z"], coord["y"], coord["x"])
    xa[(core,) + mine] = jnp.concatenate([ffn_in, meta], axis=1)

    def width(p):
        off, n, order = PARTS[p]
        return pl.ds(off, n + META if p == 2 else n)

    def moved(p, phase, k, at, to, sems):
        send, recv = sems
        ref = xa.at[(core,) + at + (ALL, width(p))]
        return pltpu.make_async_remote_copy(
            src_ref=ref, dst_ref=ref, send_sem=send.at[p, phase, k], recv_sem=recv.at[p, phase, k],
            device_id=(to,), device_id_type=MESH,
        )

    def over(p, k, at, half):
        ref = xa.at[(half,) + at + (ALL, width(p))]
        return pltpu.make_async_remote_copy(
            src_ref=ref, dst_ref=ref, send_sem=dx_send.at[p, k], recv_sem=dx_recv.at[p, k],
            device_id=(partner,), device_id_type=MESH,
        )

    arrivals = {}
    for phase in range(3):
        for p in range(3):
            order = PARTS[p][2]
            if phase > 0:
                for copy in arrivals[p, phase - 1]:
                    copy.wait_recv()
            fixed = {axis: coord[axis] for axis in order[phase:]}
            axis = order[phase]
            arrivals[p, phase] = []
            for k in (1, 2, 3):
                to, there = along(axis, k)
                copy = moved(p, phase, k - 1, pick(**fixed), to, (ag_send, ag_recv))
                copy.start()
                sent.append(copy)
                back = lax.rem(coord[axis] + 4 - k, 4)
                arrivals[p, phase].append(
                    moved(p, phase, k - 1, pick(**{**fixed, axis: back}), to, (ag_send, ag_recv))
                )
            if phase == 2:
                copy = over(p, 0, pick(**fixed), core)
                copy.start()
                sent.append(copy)
    for k in (1, 2, 3):
        for p in range(3):
            axis = PARTS[p][2][2]
            arrivals[p, 2][k - 1].wait_recv()
            back = lax.rem(coord[axis] + 4 - k, 4)
            copy = over(p, k, pick(**{axis: back}), core)
            copy.start()
            sent.append(copy)

    def settle(half):
        def body(z, carry):
            rows = pl.ds(pl.multiple_of(z * 64, 64), 64)
            xf[half, rows, :] = xa[half, z].reshape(64, D + META)
            return carry

        lax.fori_loop(0, 4, body, 0)

    settle(core)
    for p in range(3):
        axis = PARTS[p][2][2]
        for k in range(4):
            back = lax.rem(coord[axis] + 4 - k, 4)
            over(p, k, pick(**{axis: back}), 1 - core).wait_recv()
    settle(1 - core)

    lane = lax.broadcasted_iota(jnp.int32, (512, META), 1)
    scales = xf[:, :, D:].reshape(512, META).astype(F32)
    route = jnp.sum(jnp.where((lane == block) | (lane == block + 8), scales, 0.0), axis=1, keepdims=True)
    dense = jnp.sum(jnp.where((lane == 16) | (lane == 17), scales, 0.0), axis=1, keepdims=True)
    for copy in w_loads:
        copy.wait()

    def expert(n, carry):
        both = jnp.dot(xf[:, :, :D].reshape(512, D), w1[n], preferred_element_type=F32)
        g, u = both[:, :128], both[:, 128:]
        act[n] = (g * jax.nn.sigmoid(g) * u * route).astype(BF)
        return carry

    lax.fori_loop(0, 3, expert, 0)
    for copy in own_loads:
        copy.wait()
    for k in range(1, 8):
        back = lax.rem(block + 8 - k, 8)
        cols = pl.ds(pl.multiple_of(back * 256, 256), 256)
        for j, (src, dst) in enumerate(
            (
                (ds.at[block, pl.ds(0, 2)], dgu.at[:, pl.ds(0, PAD), cols]),
                (ds.at[block, 2], w2.at[pl.ds(HID, PAD), cols]),
            )
        ):
            pltpu.make_async_remote_copy(
                src_ref=src, dst_ref=dst, send_sem=ds_send.at[j, k - 1], recv_sem=ds_recv.at[j, k - 1],
                device_id=(back * 16 + column,), device_id_type=MESH,
            ).wait_recv()
    both = lax.dot_general(xf[:, :, :D].reshape(512, D), dgu[...].reshape(256, D), NT, preferred_element_type=F32)
    g, u = both[:, :128], both[:, 128:]
    act[3] = (g * jax.nn.sigmoid(g) * u * dense).astype(BF)

    def columns(p):
        return pl.ds(PARTS[p][0], PARTS[p][1])

    def product(half, p):
        rows = pl.ds(pl.multiple_of(half * 256, 256), 256)
        left = jnp.concatenate([act[n, rows, :] for n in range(4)], axis=1)
        return jnp.dot(left, w2[:, columns(p)], preferred_element_type=F32)

    def swap(p):
        at = (ALL, ALL, ALL, ALL, columns(p))
        return pltpu.make_async_remote_copy(
            src_ref=pd.at[at], dst_ref=rs0.at[at], send_sem=rd_send.at[p], recv_sem=rd_recv.at[p],
            device_id=(partner,), device_id_type=MESH,
        )

    def multiply(p):
        n = PARTS[p][1]
        pd[:, :, :, :, columns(p)] = product(1 - core, p).astype(BF).reshape(4, 4, 4, 4, n)
        copy = swap(p)
        copy.start()
        sent.append(copy)
        pf[:, columns(p)] = product(core, p)

    def hop(p, phase):
        axis = PARTS[p][2][2 - phase]
        copies = []
        for k in (1, 2, 3):
            to, there = along(axis, k)
            if phase == 0:
                src = sb1.at[pick(**{axis: there}) + (ALL, columns(p))]
                dst = rb1.at[k - 1, :, :, :, columns(p)]
            elif phase == 1:
                order = PARTS[p][2]
                first = "zyx".index(order[1]) < "zyx".index(order[0])
                at = (there, ALL) if first else (ALL, there)
                src = sb2.at[at + (ALL, columns(p))]
                dst = rb2.at[k - 1, :, :, columns(p)]
            else:
                src = sb3.at[there, :, columns(p)]
                dst = rb3.at[k - 1, :, columns(p)]
            copy = pltpu.make_async_remote_copy(
                src_ref=src, dst_ref=dst, send_sem=rs_send.at[p, phase, k - 1], recv_sem=rs_recv.at[p, phase, k - 1],
                device_id=(to,), device_id_type=MESH,
            )
            copy.start()
            copies.append(copy)
            sent.append(copy)
        return copies

    flights = {}

    def begin(p):
        n = PARTS[p][1]
        swap(p).wait_recv()
        far = rs0[:, :, :, :, columns(p)].reshape(256, n).astype(F32)
        sb1[:, :, :, :, columns(p)] = (pf[:, columns(p)] + far).astype(BF).reshape(4, 4, 4, 4, n)
        flights[p] = hop(p, 0)

    multiply(0)
    multiply(1)
    begin(0)
    multiply(2)
    begin(1)
    begin(2)
    for p in range(3):
        n = PARTS[p][1]
        axis = PARTS[p][2][2]
        for copy in flights[p]:
            copy.wait_recv()
        total = sb1[pick(**{axis: coord[axis]}) + (ALL, columns(p))].reshape(64, n).astype(F32)
        for k in range(3):
            total += rb1[k, :, :, :, columns(p)].reshape(64, n).astype(F32)
        sb2[:, :, :, columns(p)] = total.astype(BF).reshape(4, 4, 4, n)
        flights[p] = hop(p, 1)
    for p in range(3):
        n = PARTS[p][1]
        order = PARTS[p][2]
        for copy in flights[p]:
            copy.wait_recv()
        first = "zyx".index(order[1]) < "zyx".index(order[0])
        at = (coord[order[1]], ALL) if first else (ALL, coord[order[1]])
        total = sb2[at + (ALL, columns(p))].reshape(16, n).astype(F32)
        for k in range(3):
            total += rb2[k, :, :, columns(p)].reshape(16, n).astype(F32)
        sb3[:, :, columns(p)] = total.astype(BF).reshape(4, 4, n)
        flights[p] = hop(p, 2)
    for p in range(3):
        off, n, order = PARTS[p]
        for copy in flights[p]:
            copy.wait_recv()
        total = sb3[coord[order[0]], :, columns(p)].astype(F32)
        for k in range(3):
            total += rb3[k, :, columns(p)].astype(F32)
        out[:, off : off + n] = (hidden[:, off : off + n] + total).astype(BF)
    for copy in sent:
        copy.wait_send()


def per_device(
    tokens, lengths, cache_keys, cache_values, query_w, key_w, value_w, out_w, mix_lambda, head_gain,
    attn_gain, ffn_gain, routes, route_weights, exp_gate, exp_up, exp_down,
    dense_gate, dense_up, dense_down, branch_gate,
):
    def vm(*shape, dtype=BF):
        return pltpu.VMEM(shape, dtype)

    dma = pltpu.SemaphoreType.DMA
    scratch = [
        vm(4, D), vm(1, 4, dtype=jnp.int32), vm(4, 2048, 128), vm(4, 2048, 128),
        vm(D, 1024), vm(D, 256), vm(D, 256), vm(1024, D),
        vm(1, 8, dtype=F32), vm(1, 128, dtype=F32), vm(1, D, dtype=F32), vm(1, D, dtype=F32),
        vm(2, 4, dtype=jnp.int32), vm(2, 4, dtype=F32), vm(1, D),
        vm(3, D, 256), vm(512, D), vm(2, 128, D), vm(256, 352), vm(256, 352), vm(352, 256),
        vm(8, 3, PAD, 256), vm(8, 4, 128, dtype=F32), vm(4, 8, 128, dtype=F32),
        vm(2, 4, 4, 4, 4, D + META), vm(2, 256, D + META), vm(4, 512, 128),
        vm(4, 4, 4, 4, D), vm(4, 4, 4, 4, D), vm(256, D, dtype=F32), vm(4, 4, 4, 4, D),
        vm(3, 4, 4, 4, D), vm(4, 4, 4, D), vm(3, 4, 4, D), vm(4, 4, D), vm(3, 4, D),
        dma((21,)), dma((12,)), dma((7,)), dma((2,)),
        dma((2, 7)), dma((2, 7)), dma((3, 3, 3)), dma((3, 3, 3)), dma((3, 4)), dma((3, 4)),
        dma((3,)), dma((3,)), dma((3, 3, 3)), dma((3, 3, 3)),
    ]
    return pl.pallas_call(
        kernel,
        out_shape=(
            jax.ShapeDtypeStruct((4, D), BF),
            jax.ShapeDtypeStruct((4, 256), BF),
            jax.ShapeDtypeStruct((4, 256), BF),
        ),
        in_specs=[pl.BlockSpec(memory_space=pl.ANY)] * 21,
        out_specs=[pl.BlockSpec(memory_space=pltpu.VMEM)] * 3,
        scratch_shapes=scratch,
        compiler_params=pltpu.CompilerParams(
            collective_id=0, has_side_effects=True, vmem_limit_bytes=56 * 1024 * 1024
        ),
        name="layer",
    )(
        tokens, lengths.reshape(1, 4), cache_keys.reshape(4, 2048, 128), cache_values.reshape(4, 2048, 128),
        query_w, key_w, value_w, out_w, mix_lambda.reshape(1, 8), head_gain.reshape(1, 128),
        attn_gain.reshape(1, D), ffn_gain.reshape(1, D), routes.T, route_weights.T,
        exp_gate, exp_up, exp_down, dense_gate, dense_up, dense_down, branch_gate.reshape(1, D),
    )


def solution(mesh):
    placed = (
        P("ep", None), P("ep"), P("ep", None, None, None), P("ep", None, None, None),
        P(), P(), P(), P(), P(), P(), P(), P(),
        P("ep", None), P("ep", None), P(None, "ep"), P(None, "ep"), P("ep", None),
        P("ep", None, None), P("ep", None, None), P("ep", None, None), P(),
    )
    return jax.shard_map(
        per_device,
        mesh=mesh,
        in_specs=placed,
        out_specs=(P("ep", None), P("ep", None), P("ep", None)),
        check_vma=False,
    )
```

time: 200 us -> 62.2 us (0.31)
  waiting for transfers between devices: 66.9 us -> 0 us
  Pallas kernels: 0 us -> 52.7 us
  starting transfers between devices: 41.2 us -> 0 us
  local copies, waits for them, and re-layouts: 37.7 us -> 8.59 us
  matrix products: 21 us -> 0 us
  other arithmetic: 17.1 us -> 0 us
  between operations: 14.5 us -> 0.64 us
    pallas_call x0 -> x1, Pallas kernels: none -> 52.7 us  [per_device(): pl.pallas_call(kernel, out_shape=(jax.ShapeDtypeStruct((4, D), BF), jax.S...]
    all_to_all x6 -> x0, waiting for transfers between devices: 48.1 us -> none  [the longest x1 18.7 us: per_device(): lax.all_to_all(outgoing, 'ep', split_axis=0, concat_axis=0, tiled=True)]
    all_to_all x6 -> x0, starting transfers between devices: 41.2 us -> none  [the longest x1 11.9 us: per_device(): lax.all_to_all(outgoing, 'ep', split_axis=0, concat_axis=0, tiled=True)]
    dot_general x17 -> x0, matrix products: 21 us -> none  [the longest x1 4.37 us: swiglu_rows(): return jnp.dot(act, w_down, preferred_element_type=jnp.float32)]
    all_gather x1 -> x0, waiting for transfers between devices: 18.9 us -> none  [per_device(): all_rows = lax.all_gather(ffn_in, 'ep', axis=0, tiled=True)]
    split x2 -> x0, other arithmetic: 9.14 us -> none  [exchange_in_pieces(): jnp.split(tiles, cut_rows(tiles.shape[cut], pieces), axis=cut)]
    unnamed x46 -> x5, local copies, waits for them, and re-layouts: 15.6 us -> 7.3 us
    slice x2 -> x0, local copies, waits for them, and re-layouts: 6.83 us -> none  [the longest x1 6.76 us: per_device(): cache_keys[..., half:]]
  transfers between devices with their start and end apart: 7 -> 0, of which waited for: 6 -> 0; matrix products, arithmetic and copies ran while one was open for 27% -> 0% of each run, Pallas kernels for 0% -> 0%
where the time goes in v1:
time: 62.2 us; the launch traced here: 62 us
  Pallas kernels  52.7 us (85%)
  local copies, waits for them, and re-layouts  8.59 us (14%)
  between operations  0.64 us (1%)
    pallas_call x1, Pallas kernels, per_device(): pl.pallas_call(kernel, out_shape=(jax.ShapeDtypeStruct((4, D), BF), jax.S...  52.7 us
    unnamed x5, local copies, waits for them, and re-layouts  7.3 us
    reshape x1, local copies, waits for them, and re-layouts, per_device(): branch_gate.reshape(1, D)  1.29 us

profile of v1, /device:TPU:0, one launch (start us, length us, event | category | flops | bytes accessed | tf_op | source)
XLA Modules:
  0.0 62.0 jit_solution(13824993637501716011)
XLA Ops:
  0.6 1.3 %reshape.37.branch_gate = bf16[1,2048]{1,0:T(2,128)(2,1)} reshape(bf16[2048]{0:T(1024)(128)(2,1)} %param.41) | data formatting | bytes 8192 | tf_op jit(solution)/shard_map/reshape | solution.py:462
  1.9 1.7 %copy.24.dense_gate = bf16[1,256,352]{2,1,0:T(8,128)(2,1)} copy(bf16[1,256,352]{1,2,0:T(8,128)(2,1)} %param.38) | data formatting | bytes 360448 | tf_op args[17]
  3.7 1.7 %copy.25.dense_up = bf16[1,256,352]{2,1,0:T(8,128)(2,1)} copy(bf16[1,256,352]{1,2,0:T(8,128)(2,1)} %param.39) | data formatting | bytes 360448 | tf_op args[18]
  5.4 52.7 %layer.1 = (bf16[4,2048]{1,0:T(4,128)(2,1)}, bf16[4,256]{1,0:T(4,128)(2,1)}, bf16[4,256]{1,0:T(4,128)(2,1)}) custom-call(bf16[4,2048]{1,0:T(4,128)(2,1)} %tokens.1, s32[1,4]{1,0:T(1,128)} %bitcast.15, bf16[4,2048,128]{2,1,0:T(8,128)(2,1)} %bitcast.9, bf16[4,2048,128]{2,1,0:T(8,128)(2,1)} %bitcast.10, bf16[2048,1024]{1,0:T(8,128)(2,1)} %query_w.1, ...), custom_call_target="tpu_custom_call" | custom-call | tf_op jit(solution)/shard_map/layer/pallas_call | solution.py:444
  58.1 1.3 %copy.29 = bf16[4,2048]{1,0:T(4,128)(2,1)} copy(bf16[4,2048]{1,0:T(4,128)(2,1)} %get-tuple-element.6) | data formatting | bytes 32768
  59.5 1.3 %copy.30 = bf16[4,256]{1,0:T(4,128)(2,1)} copy(bf16[4,256]{1,0:T(4,128)(2,1)} %get-tuple-element.7) | data formatting | bytes 4096
  60.7 1.2 %copy.31 = bf16[4,256]{1,0:T(4,128)(2,1)} copy(bf16[4,256]{1,0:T(4,128)(2,1)} %get-tuple-element.8) | data formatting | bytes 4096

commit v2 on v1

--- a/solution.py
+++ b/solution.py
@@ -115,9 +115,8 @@
         ],
         axis=0,
     ).astype(BF)
-    ds[:, 0] = lax.dot_general(choose, dg_v[...], NT, preferred_element_type=F32).astype(BF).reshape(8, PAD, 256)
-    ds[:, 1] = lax.dot_general(choose, du_v[...], NT, preferred_element_type=F32).astype(BF).reshape(8, PAD, 256)
-    ds[:, 2] = jnp.dot(choose, dd_v[...], preferred_element_type=F32).astype(BF).reshape(8, PAD, 256)
+    for j, tile in enumerate((dg_v, du_v, dd_v)):
+        ds[:, j] = jnp.dot(choose, tile[...], preferred_element_type=F32).astype(BF).reshape(8, PAD, 256)
 
     small[0].wait()
     small[1].wait()
@@ -204,9 +203,11 @@
     ffn_in = (
         hidden * lax.rsqrt(jnp.mean(hidden * hidden, axis=1, keepdims=True) + 1e-6) * fg_v[...]
     ).astype(BF)
-    gate = jax.nn.sigmoid(
-        jnp.sum(ffn_in.astype(F32) * bg_v[...].astype(F32), axis=1, keepdims=True)
-    )
+    gate_w = bg_v[...].astype(F32)
+    toward = jnp.zeros((4, 128), F32)
+    for j in range(16):
+        toward += ffn_in[:, j * 128 : (j + 1) * 128].astype(F32) * gate_w[j : j + 1]
+    gate = jax.nn.sigmoid(jnp.sum(toward, axis=1, keepdims=True))
     lane4 = lax.broadcasted_iota(jnp.int32, (4, META), 1)
     expert4 = lax.rem(lane4, 8)
     scale = jnp.where(lane4 < 16, 0.0, gate)
@@ -431,8 +432,8 @@
         vm(4, D), vm(1, 4, dtype=jnp.int32), vm(4, 2048, 128), vm(4, 2048, 128),
         vm(D, 1024), vm(D, 256), vm(D, 256), vm(1024, D),
         vm(1, 8, dtype=F32), vm(1, 128, dtype=F32), vm(1, D, dtype=F32), vm(1, D, dtype=F32),
-        vm(2, 4, dtype=jnp.int32), vm(2, 4, dtype=F32), vm(1, D),
-        vm(3, D, 256), vm(512, D), vm(2, 128, D), vm(256, 352), vm(256, 352), vm(352, 256),
+        vm(2, 4, dtype=jnp.int32), vm(2, 4, dtype=F32), vm(16, 128),
+        vm(3, D, 256), vm(512, D), vm(2, 128, D), vm(352, 256), vm(352, 256), vm(352, 256),
         vm(8, 3, PAD, 256), vm(8, 4, 128, dtype=F32), vm(4, 8, 128, dtype=F32),
         vm(2, 4, 4, 4, 4, D + META), vm(2, 256, D + META), vm(4, 512, 128),
         vm(4, 4, 4, 4, D), vm(4, 4, 4, 4, D), vm(256, D, dtype=F32), vm(4, 4, 4, 4, D),
@@ -443,11 +444,7 @@
     ]
     return pl.pallas_call(
         kernel,
-        out_shape=(
-            jax.ShapeDtypeStruct((4, D), BF),
-            jax.ShapeDtypeStruct((4, 256), BF),
-            jax.ShapeDtypeStruct((4, 256), BF),
-        ),
+        out_shape=(vm(4, D), vm(4, 256), vm(4, 256)),
         in_specs=[pl.BlockSpec(memory_space=pl.ANY)] * 21,
         out_specs=[pl.BlockSpec(memory_space=pltpu.VMEM)] * 3,
         scratch_shapes=scratch,
@@ -459,7 +456,7 @@
         tokens, lengths.reshape(1, 4), cache_keys.reshape(4, 2048, 128), cache_values.reshape(4, 2048, 128),
         query_w, key_w, value_w, out_w, mix_lambda.reshape(1, 8), head_gain.reshape(1, 128),
         attn_gain.reshape(1, D), ffn_gain.reshape(1, D), routes.T, route_weights.T,
-        exp_gate, exp_up, exp_down, dense_gate, dense_up, dense_down, branch_gate.reshape(1, D),
+        exp_gate, exp_up, exp_down, dense_gate.transpose(0, 2, 1), dense_up.transpose(0, 2, 1), dense_down, branch_gate.reshape(16, 128),
     )
 
 

time: 62.2 us -> 54.7 us (0.88)
  local copies, waits for them, and re-layouts: 8.59 us -> 1.76 us
    unnamed x5 -> x3, local copies, waits for them, and re-layouts: 7.3 us -> 1.76 us
    reshape x1 -> x0, local copies, waits for them, and re-layouts: 1.29 us -> none  [per_device(): branch_gate.reshape(1, D)]
where the time goes in v2:
time: 54.7 us; the launch traced here: 54.6 us
  Pallas kernels  52.2 us (95%)
  local copies, waits for them, and re-layouts  1.76 us (3%)
  between operations  0.65 us (1%)
    pallas_call x1, Pallas kernels, per_device(): pl.pallas_call(kernel, out_shape=(vm(4, D), vm(4, 256), vm(4, 256)), in_s...  52.2 us
    unnamed x3, local copies, waits for them, and re-layouts  1.76 us

profile of v2, /device:TPU:0, one launch (start us, length us, event | category | flops | bytes accessed | tf_op | source)
XLA Modules:
  0.0 54.6 jit_solution(7233851987205579292)
XLA Ops:
  0.6 52.2 %layer.1 = (bf16[4,2048]{1,0:T(4,128)(2,1)S(1)}, bf16[4,256]{1,0:T(4,128)(2,1)S(1)}, bf16[4,256]{1,0:T(4,128)(2,1)S(1)}) custom-call(bf16[4,2048]{1,0:T(4,128)(2,1)} %tokens.1, s32[1,4]{1,0:T(1,128)} %bitcast.21, bf16[4,2048,128]{2,1,0:T(8,128)(2,1)} %bitcast.12, bf16[4,2048,128]{2,1,0:T(8,128)(2,1)} %bitcast.13, bf16[2048,1024]{1,0:T(8,128)(2,1)} %query_w.1, ...), custom_call_target="tpu_custom_call" | custom-call | tf_op jit(solution)/shard_map/layer/pallas_call | solution.py:445
  52.8 0.6 %copy.27 = bf16[4,2048]{1,0:T(4,128)(2,1)} copy(bf16[4,2048]{1,0:T(4,128)(2,1)S(1)} %get-tuple-element.3) | data formatting | bytes 32768
  53.4 0.6 %copy.28 = bf16[4,256]{1,0:T(4,128)(2,1)} copy(bf16[4,256]{1,0:T(4,128)(2,1)S(1)} %get-tuple-element.4) | data formatting | bytes 4096
  54.0 0.6 %copy.29 = bf16[4,256]{1,0:T(4,128)(2,1)} copy(bf16[4,256]{1,0:T(4,128)(2,1)S(1)} %get-tuple-element.5) | data formatting | bytes 4096

commit v3 on v2

v3 whole, which is shorter than its diff:
```python
import jax
import jax.numpy as jnp
from jax import lax
from jax.experimental import pallas as pl
from jax.experimental.pallas import tpu as pltpu
from jax.sharding import PartitionSpec as P

BF = jnp.bfloat16
F32 = jnp.float32
MESH = pl.DeviceIdType.MESH
ALL = slice(None)
D = 2048
META = 128
HID = 384
PAD = 48
PARTS = ((0, 768, "xyz"), (768, 640, "yzx"), (1408, 640, "zxy"))
STRIDE = {"x": 2, "y": 8, "z": 32}
NT = (((1,), (1,)), ((), ()))


def pick(**at):
    return tuple(at.get(axis, ALL) for axis in "zyx")


def to_col(row):
    n = row.shape[1]
    same = lax.broadcasted_iota(jnp.int32, (n, n), 0) == lax.broadcasted_iota(jnp.int32, (n, n), 1)
    return jnp.sum(jnp.where(same, jnp.broadcast_to(row, (n, n)), 0.0), axis=1, keepdims=True)


def kernel(
    tokens, lengths, keys, values, query_w, key_w, value_w, out_w, mix_lambda, head_gain,
    attn_gain, ffn_gain, routes, route_weights, exp_gate, exp_up, exp_down,
    dense_gate, dense_up, dense_down, branch_gate,
    out, new_keys, new_values,
    tok_v, len_v, k_v, v_v, wq_v, wk_v, wv_v, wo_v, lam_v, hg_v, ag_v, fg_v, rt_v, rw_v, bg_v,
    w1, w2, dgu, qs, hs, xa, xf, act, pd, rs0, sb1, rb1, sb2, rb2,
    load_sem, qkv_sem, w_sem, ds_sem, dd_sem, ag_send, ag_recv, dx_recv, rd_recv, rs_send, rs1_recv, rs2_recv,
):
    me = lax.axis_index("ep")
    core = lax.rem(me, 2)
    coord = {
        "x": lax.rem(lax.div(me, 2), 4),
        "y": lax.rem(lax.div(me, 8), 4),
        "z": lax.div(me, 32),
    }
    block = lax.div(me, 16)
    column = lax.rem(me, 16)
    partner = me + 1 - 2 * core

    def along(axis, k):
        there = lax.rem(coord[axis] + k, 4)
        return me + (there - coord[axis]) * STRIDE[axis], there

    def across(one, k, two, l):
        first, second = lax.rem(coord[one] + k, 4), lax.rem(coord[two] + l, 4)
        to = me + (first - coord[one]) * STRIDE[one] + (second - coord[two]) * STRIDE[two]
        return to, first, second

    barrier = pltpu.get_barrier_semaphore()
    friends = [partner]
    for axis in "xyz":
        for k in (1, 2, 3):
            friends.append(along(axis, k)[0])
    for one, two in ("xy", "yz", "zx"):
        for k in (1, 2, 3):
            for l in (1, 2, 3):
                friends.append(across(one, k, two, l)[0])
    for friend in friends:
        pl.semaphore_signal(barrier, inc=1, device_id=(friend,), device_id_type=MESH)

    def remote(src, dst, send, recv, to):
        return pltpu.make_async_remote_copy(
            src_ref=src, dst_ref=dst, send_sem=send, recv_sem=recv, device_id=(to,), device_id_type=MESH
        )

    def load(src, dst, sem):
        copy = pltpu.make_async_copy(src, dst, sem)
        copy.start()
        return copy

    def load_all(pairs, sem):
        return [load(src, dst, sem) for src, dst in pairs]

    def finish(copies):
        for copy in copies:
            copy.wait()

    first = [load(tokens, tok_v, load_sem.at[0]), load(attn_gain, ag_v, load_sem.at[1])]
    step = D // 4
    qkv_loads = []
    for i in range(4):
        rows = pl.ds(i * step, step)
        qkv_loads.append(
            [
                load(query_w.at[rows], wq_v.at[rows], qkv_sem.at[i, 0]),
                load(key_w.at[rows], wk_v.at[rows], qkv_sem.at[i, 1]),
                load(value_w.at[rows], wv_v.at[rows], qkv_sem.at[i, 2]),
            ]
        )
    small = [
        load(src, dst, load_sem.at[5 + i])
        for i, (src, dst) in enumerate(
            (
                (lengths, len_v), (mix_lambda, lam_v), (head_gain, hg_v),
                (ffn_gain, fg_v), (routes, rt_v), (route_weights, rw_v), (branch_gate, bg_v),
            )
        )
    ]
    k_load = load(keys, k_v, load_sem.at[12])
    dgu[:, PAD:, :] = jnp.zeros((2, 128 - PAD, D), BF)
    w2[HID + PAD :, :] = jnp.zeros((128 - PAD, D), BF)

    own_cols = pl.ds(pl.multiple_of(block * 256, 256), 256)

    def units(there):
        return pl.ds(pl.multiple_of(lax.div(there, 2) * 88 + lax.rem(there, 2) * 40, 8), PAD)

    def hand_out(pairs, sems):
        for k in range(1, 8):
            there = lax.rem(block + k, 8)
            for src, dst in pairs:
                remote(src.at[0, units(there)], dst, sems.at[0], sems.at[1], there * 16 + column).start()

    up_pairs = (
        (dense_gate, dgu.at[0, pl.ds(0, PAD), own_cols]),
        (dense_up, dgu.at[1, pl.ds(0, PAD), own_cols]),
    )
    down_pairs = ((dense_down, w2.at[pl.ds(HID, PAD), own_cols]),)
    own_loads = [
        load(src.at[0, units(block)], dst, load_sem.at[2 + i])
        for i, (src, dst) in enumerate(up_pairs + down_pairs)
    ]
    finish(first)
    x = tok_v[...].astype(F32)
    normed = (x * lax.rsqrt(jnp.mean(x * x, axis=1, keepdims=True) + 1e-6) * ag_v[...]).astype(BF)

    query = jnp.zeros((4, 1024), F32)
    key = jnp.zeros((4, 256), F32)
    value = jnp.zeros((4, 256), F32)
    for i in range(4):
        finish(qkv_loads[i])
        if i == 0:
            v_load = load(values, v_v, load_sem.at[13])
        if i == 2:
            o_load = load(out_w, wo_v, load_sem.at[14])
            pl.semaphore_wait(barrier, len(friends))
            hand_out(up_pairs, ds_sem)
        part = normed[:, i * step : (i + 1) * step]
        rows = pl.ds(i * step, step)
        query += jnp.dot(part, wq_v[rows, :], preferred_element_type=F32)
        key += jnp.dot(part, wk_v[rows, :], preferred_element_type=F32)
        value += jnp.dot(part, wv_v[rows, :], preferred_element_type=F32)
    key = key.astype(BF)
    value = value.astype(BF)
    new_keys[...] = key
    new_values[...] = value
    key = key.astype(F32)
    value = value.astype(F32)
    query = query.astype(BF).astype(F32)
    for h in range(8):
        qs[h] = query[:, h * 128 : (h + 1) * 128]

    w_loads = []
    for n in range(3):
        cols = pl.ds(n * 128, 128)
        w_loads.append(load(exp_gate.at[:, cols], w1.at[n, :, pl.ds(0, 128)], w_sem.at[2 * n]))
        w_loads.append(load(exp_up.at[:, cols], w1.at[n, :, pl.ds(128, 128)], w_sem.at[2 * n + 1]))
    w_loads.append(load(exp_down, w2.at[pl.ds(0, HID)], w_sem.at[6]))
    finish(small)
    k_load.wait()
    lam = to_col(lam_v[...])
    row8 = lax.broadcasted_iota(jnp.int32, (8, 128), 0)
    lane8 = lax.broadcasted_iota(jnp.int32, (8, 128), 1)
    row16 = lax.rem(lax.broadcasted_iota(jnp.int32, (16, 2048), 0), 8)
    spot = lax.broadcasted_iota(jnp.int32, (16, 2048), 1)
    place = jnp.where(lax.rem(spot, 2) == lax.div(row16, 4), spot, 2 * D)
    scores = []
    owns = []
    for s in range(4):
        heads_q = qs[:, s, :]
        q16 = jnp.concatenate(
            [jnp.where(lane8 < 64, heads_q, 0.0), jnp.where(lane8 >= 64, heads_q, 0.0)], axis=0
        )
        own_key = jnp.where(row8 < 4, key[s : s + 1, :128], key[s : s + 1, 128:])
        score = lax.dot_general(q16.astype(BF), k_v[s], NT, preferred_element_type=F32) * 0.125
        scores.append(jnp.where(place < 2 * len_v[0:1, s : s + 1], score, -jnp.inf))
        owns.append(
            jnp.sum(q16 * jnp.concatenate([own_key, own_key], axis=0), axis=1, keepdims=True) * 0.125
        )
    weights = []
    own_weights = []
    for s in range(4):
        largest = jnp.maximum(jnp.max(scores[s], axis=1, keepdims=True), owns[s])
        raised = jnp.exp(scores[s] - largest)
        own_raised = jnp.exp(owns[s] - largest)
        share = 1.0 / (jnp.sum(raised, axis=1, keepdims=True) + own_raised)
        first_share, second_share = share[:8], lam * share[8:]
        weights.append((raised[:8] * first_share - raised[8:] * second_share).astype(BF))
        own_weights.append(
            (own_raised[:8] * first_share - own_raised[8:] * second_share).astype(BF).astype(F32)
        )
    v_load.wait()
    for s in range(4):
        own_value = jnp.where(row8 < 4, value[s : s + 1, :128], value[s : s + 1, 128:])
        mixed = jnp.dot(weights[s], v_v[s], preferred_element_type=F32) + own_weights[s] * own_value
        hs[s] = mixed * lax.rsqrt(jnp.mean(mixed * mixed, axis=1, keepdims=True) + 1e-5) * hg_v[...]
    heads = jnp.concatenate([hs[:, h, :] for h in range(8)], axis=1).astype(BF)
    o_load.wait()
    hidden = x + jnp.dot(heads, wo_v[...], preferred_element_type=F32)
    ffn_in = (
        hidden * lax.rsqrt(jnp.mean(hidden * hidden, axis=1, keepdims=True) + 1e-6) * fg_v[...]
    ).astype(BF)
    gate_w = bg_v[...].astype(F32)
    toward = jnp.zeros((4, 128), F32)
    for j in range(16):
        toward += ffn_in[:, j * 128 : (j + 1) * 128].astype(F32) * gate_w[j : j + 1]
    gate = jax.nn.sigmoid(jnp.sum(toward, axis=1, keepdims=True))
    lane4 = lax.broadcasted_iota(jnp.int32, (4, META), 1)
    expert4 = lax.rem(lane4, 8)
    scale = jnp.where(lane4 < 16, 0.0, gate)
    for j in range(2):
        named = to_col(rt_v[j : j + 1, :].astype(F32)).astype(jnp.int32)
        scale += jnp.where((expert4 == named) & (lane4 < 16), to_col(rw_v[j : j + 1, :]), 0.0)
    upper = scale.astype(BF).astype(F32)
    meta = jnp.where(
        (lane4 < 8) | (lane4 == 16), upper, jnp.where((lane4 < 16) | (lane4 == 17), scale - upper, 0.0)
    ).astype(BF)
    mine = (coord["z"], coord["y"], coord["x"])
    xa[(core,) + mine] = jnp.concatenate([ffn_in, meta], axis=1)

    def width(p):
        off, n, order = PARTS[p]
        return pl.ds(off, n + META if p == 2 else n)

    def piece(p, half, **at):
        return xa.at[(half,) + pick(**at) + (ALL, width(p))]

    def behind(axis, k):
        return lax.rem(coord[axis] + 4 - k, 4)

    for line in (2, 1, 3, 0):
        for k in (2, 1, 3, 0):
            for p in range(3):
                a1, a2, a3 = PARTS[p][2]
                if line or k:
                    ref = piece(p, core, **coord)
                    send = ag_send.at[1 if line else 0]
                    remote(ref, ref, send, ag_recv.at[p, 0, line], across(a1, k, a2, line)[0]).start()
    for line in (0, 1, 3, 2):
        for p in range(3):
            a1, a2, a3 = PARTS[p][2]
            ref = piece(p, core, **{a2: behind(a2, line), a3: coord[a3]})
            came = ref if line else piece(p, core, **{a1: pl.ds(0, 3), a2: coord[a2], a3: coord[a3]})
            remote(came, came, ag_send.at[1], ag_recv.at[p, 0, line], partner).wait_recv()
            for k in (2, 1, 3):
                remote(ref, ref, ag_send.at[2], ag_recv.at[p, 1, line], along(a3, k)[0]).start()
    hand_out(down_pairs, dd_sem)
    for line in (0, 1, 3, 2):
        for p in range(3):
            a1, a2, a3 = PARTS[p][2]
            three = piece(p, core, **{a2: behind(a2, line), a3: pl.ds(0, 3)})
            remote(three, three, ag_send.at[2], ag_recv.at[p, 1, line], partner).wait_recv()
            ref = piece(p, core, **{a2: behind(a2, line)})
            remote(ref, ref, ag_send.at[3], dx_recv.at[p, line], partner).start()

    def settle(half):
        def body(z, carry):
            rows = pl.ds(pl.multiple_of(z * 64, 64), 64)
            xf[half, rows, :] = xa[half, z].reshape(64, D + META)
            return carry

        lax.fori_loop(0, 4, body, 0)

    for copy in w_loads:
        copy.wait()
    finish(own_loads)
    came = dgu.at[:, pl.ds(0, PAD), pl.ds(0, 7 * 256)]
    remote(came, came, ds_sem.at[0], ds_sem.at[1], partner).wait_recv()
    lane = lax.broadcasted_iota(jnp.int32, (256, META), 1)
    spare = (lane >= 8 * lax.rem(block, 2)) & (lane < PAD)

    def hidden_units(half):
        settle(half)
        scales = xf[half, :, D:].astype(F32)
        route = jnp.sum(jnp.where((lane == block) | (lane == block + 8), scales, 0.0), axis=1, keepdims=True)
        dense = jnp.sum(jnp.where((lane == 16) | (lane == 17), scales, 0.0), axis=1, keepdims=True)
        for n in range(3):
            both = jnp.dot(xf[half, :, :D], w1[n], preferred_element_type=F32)
            g, u = both[:, :128], both[:, 128:]
            act[half, :, n * 128 : (n + 1) * 128] = (g * jax.nn.sigmoid(g) * u * route).astype(BF)
        both = lax.dot_general(xf[half, :, :D], dgu[...].reshape(256, D), NT, preferred_element_type=F32)
        g, u = both[:, :128], both[:, 128:]
        act[half, :, HID:] = jnp.where(spare, g * jax.nn.sigmoid(g) * u * dense, 0.0).astype(BF)

    def partner_rows():
        for line in (0, 1, 3, 2):
            for p in range(3):
                a1, a2, a3 = PARTS[p][2]
                ref = piece(p, 1 - core, **{a2: behind(a2, line)})
                remote(ref, ref, ag_send.at[3], dx_recv.at[p, line], partner).wait_recv()

    pl.when(core == 0)(partner_rows)
    hidden_units(1)
    pl.when(core == 1)(partner_rows)
    hidden_units(0)
    came = w2.at[pl.ds(HID, PAD), pl.ds(0, 7 * 256)]
    remote(came, came, dd_sem.at[0], dd_sem.at[1], partner).wait_recv()

    def columns(p, h=None):
        off, n, order = PARTS[p]
        return pl.ds(off, n) if h is None else pl.ds(off + 256 * h, 256 if h == 0 else n - 256)

    def product(half, cols):
        return jnp.dot(act[half], w2[:, cols], preferred_element_type=F32)

    def swap(p, h):
        cols = columns(p, h)
        return remote(pd.at[:, cols], rs0.at[:, cols], rs_send.at[0], rd_recv.at[p, h], partner)

    for h in range(2):
        for p in range(3):
            cols = columns(p, h)
            pd[:, cols] = product(1 - core, cols).astype(BF)
            swap(p, h).start()
    for h in range(2):
        for p in range(3):
            a1, a2, a3 = PARTS[p][2]
            cols = columns(p, h)
            near = product(core, cols)
            swap(p, h).wait_recv()
            far = rs0[:, cols].astype(F32)
            sb1[:, :, :, :, cols] = (near + far).astype(BF).reshape(4, 4, 4, 4, cols.size)
            for k in (2, 1, 3):
                to, there = along(a3, k)
                src = sb1.at[pick(**{a3: there}) + (ALL, cols)]
                remote(src, rb1.at[k - 1, :, :, :, cols], rs_send.at[1], rs1_recv.at[p, h], to).start()

    def in_plane(p, c1, c2):
        a1, a2, a3 = PARTS[p][2]
        return (c1, c2) if "zyx".index(a1) < "zyx".index(a2) else (c2, c1)

    for h in range(2):
        for p in range(3):
            a1, a2, a3 = PARTS[p][2]
            cols = columns(p, h)
            three = rb1.at[:, :, :, :, cols]
            remote(three, three, rs_send.at[1], rs1_recv.at[p, h], partner).wait_recv()
            total = sb1[pick(**{a3: coord[a3]}) + (ALL, cols)].reshape(64, cols.size).astype(F32)
            for k in range(3):
                total += rb1[k, :, :, :, cols].reshape(64, cols.size).astype(F32)
            sb2[:, :, :, cols] = total.astype(BF).reshape(4, 4, 4, cols.size)
            for k in (2, 1, 3, 0):
                for l in (2, 1, 3, 0):
                    if k or l:
                        to, c1, c2 = across(a1, k, a2, l)
                        src = sb2.at[in_plane(p, c1, c2) + (ALL, cols)]
                        remote(src, rb2.at[k * 4 + l - 1, :, cols], rs_send.at[2], rs2_recv.at[p], to).start()
    for p in range(3):
        off, n, (a1, a2, a3) = PARTS[p]
        cols = columns(p)
        most = rb2.at[:, :, cols]
        remote(most, most, rs_send.at[2], rs2_recv.at[p], partner).wait_recv()
        total = sb2[in_plane(p, coord[a1], coord[a2]) + (ALL, cols)].astype(F32)
        for k in range(15):
            total += rb2[k, :, cols].astype(F32)
        out[:, off : off + n] = (hidden[:, off : off + n] + total).astype(BF)
    for ref, sem in (
        (dgu.at[:, pl.ds(0, PAD), pl.ds(0, 7 * 256)], ds_sem.at[0]),
        (w2.at[pl.ds(HID, PAD), pl.ds(0, 7 * 256)], dd_sem.at[0]),
        (xa.at[0, 0, 0, pl.ds(0, 3)], ag_send.at[0]),
        (xa.at[0, 0, pl.ds(0, 3)], ag_send.at[1]),
        (xa.at[0, pl.ds(0, 3)], ag_send.at[2]),
        (xa.at[0], ag_send.at[3]),
        (pd, rs_send.at[0]),
        (sb1.at[pl.ds(0, 3)], rs_send.at[1]),
        (rb2, rs_send.at[2]),
    ):
        remote(ref, ref, sem, rs2_recv.at[0], partner).wait_send()


def per_device(
    tokens, lengths, cache_keys, cache_values, query_w, key_w, value_w, out_w, mix_lambda, head_gain,
    attn_gain, ffn_gain, routes, route_weights, exp_gate, exp_up, exp_down,
    dense_gate, dense_up, dense_down, branch_gate,
):
    def vm(*shape, dtype=BF):
        return pltpu.VMEM(shape, dtype)

    dma = pltpu.SemaphoreType.DMA
    scratch = [
        vm(4, D), vm(1, 4, dtype=jnp.int32), vm(4, 2048, 128), vm(4, 2048, 128),
        vm(D, 1024), vm(D, 256), vm(D, 256), vm(1024, D),
        vm(1, 8, dtype=F32), vm(1, 128, dtype=F32), vm(1, D, dtype=F32), vm(1, D, dtype=F32),
        vm(2, 4, dtype=jnp.int32), vm(2, 4, dtype=F32), vm(16, 128),
        vm(3, D, 256), vm(512, D), vm(2, 128, D), vm(8, 4, 128, dtype=F32), vm(4, 8, 128, dtype=F32),
        vm(2, 4, 4, 4, 4, D + META), vm(2, 256, D + META), vm(2, 256, HID + 128),
        vm(256, D), vm(256, D), vm(4, 4, 4, 4, D),
        vm(3, 4, 4, 4, D), vm(4, 4, 4, D), vm(15, 4, D),
        dma((17,)), dma((4, 3)), dma((7,)), dma((2,)), dma((2,)), dma((4,)), dma((3, 2, 4)), dma((3, 4)), dma((3, 2)),
        dma((3,)), dma((3, 2)), dma((3,)),
    ]
    return pl.pallas_call(
        kernel,
        out_shape=(vm(4, D), vm(4, 256), vm(4, 256)),
        in_specs=[pl.BlockSpec(memory_space=pl.ANY)] * 21,
        out_specs=[pl.BlockSpec(memory_space=pltpu.VMEM)] * 3,
        scratch_shapes=scratch,
        compiler_params=pltpu.CompilerParams(
            collective_id=0, has_side_effects=True, vmem_limit_bytes=56 * 1024 * 1024
        ),
        name="layer",
    )(
        tokens, lengths.reshape(1, 4), cache_keys.reshape(4, 2048, 128), cache_values.reshape(4, 2048, 128),
        query_w, key_w, value_w, out_w, mix_lambda.reshape(1, 8), head_gain.reshape(1, 128),
        attn_gain.reshape(1, D), ffn_gain.reshape(1, D), routes.T, route_weights.T,
        exp_gate, exp_up, exp_down, dense_gate.transpose(0, 2, 1), dense_up.transpose(0, 2, 1), dense_down, branch_gate.reshape(16, 128),
    )


def solution(mesh):
    placed = (
        P("ep", None), P("ep"), P("ep", None, None, None), P("ep", None, None, None),
        P(), P(), P(), P(), P(), P(), P(), P(),
        P("ep", None), P("ep", None), P(None, "ep"), P(None, "ep"), P("ep", None),
        P("ep", None, None), P("ep", None, None), P("ep", None, None), P(),
    )
    return jax.shard_map(
        per_device,
        mesh=mesh,
        in_specs=placed,
        out_specs=(P("ep", None), P("ep", None), P("ep", None)),
        check_vma=False,
    )
```

time: 54.7 us -> 45.2 us (0.83)
  Pallas kernels: 52.2 us -> 42.6 us
    pallas_call x1, Pallas kernels: 52.2 us -> 42.6 us  [per_device(): pl.pallas_call(kernel, out_shape=(vm(4, D), vm(4, 256), vm(4, 256)), in_s...]
where the time goes in v3:
time: 45.2 us; the launch traced here: 45 us
  Pallas kernels  42.6 us (94%)
  local copies, waits for them, and re-layouts  1.76 us (4%)
  between operations  0.65 us (1%)
    pallas_call x1, Pallas kernels, per_device(): pl.pallas_call(kernel, out_shape=(vm(4, D), vm(4, 256), vm(4, 256)), in_s...  42.6 us
    unnamed x3, local copies, waits for them, and re-layouts  1.76 us

profile of v3, /device:TPU:0, one launch (start us, length us, event | category | flops | bytes accessed | tf_op | source)
XLA Modules:
  0.0 45.0 jit_solution(14439393857016047600)
XLA Ops:
  0.6 42.6 %layer.1 = (bf16[4,2048]{1,0:T(4,128)(2,1)S(1)}, bf16[4,256]{1,0:T(4,128)(2,1)S(1)}, bf16[4,256]{1,0:T(4,128)(2,1)S(1)}) custom-call(bf16[4,2048]{1,0:T(4,128)(2,1)} %tokens.1, s32[1,4]{1,0:T(1,128)} %bitcast.21, bf16[4,2048,128]{2,1,0:T(8,128)(2,1)} %bitcast.12, bf16[4,2048,128]{2,1,0:T(8,128)(2,1)} %bitcast.13, bf16[2048,1024]{1,0:T(8,128)(2,1)} %query_w.1, ...), custom_call_target="tpu_custom_call" | custom-call | tf_op jit(solution)/shard_map/layer/pallas_call | solution.py:403
  43.2 0.6 %copy.27 = bf16[4,2048]{1,0:T(4,128)(2,1)} copy(bf16[4,2048]{1,0:T(4,128)(2,1)S(1)} %get-tuple-element.3) | data formatting | bytes 32768
  43.9 0.6 %copy.28 = bf16[4,256]{1,0:T(4,128)(2,1)} copy(bf16[4,256]{1,0:T(4,128)(2,1)S(1)} %get-tuple-element.4) | data formatting | bytes 4096
  44.4 0.6 %copy.29 = bf16[4,256]{1,0:T(4,128)(2,1)} copy(bf16[4,256]{1,0:T(4,128)(2,1)S(1)} %get-tuple-element.5) | data formatting | bytes 4096
